TPU v7x, 256 devices: a whole 4x4x8 slice. The times are simulated.
256 devices in a mesh: sp: 32 (over z, y), tp: 8 (over x, core).
Axes of the slice: x: 4, y: 4, z: 8, core: 2. Of those that a mesh axis runs over, the one named last changes fastest.
Arguments:
- tokens: bfloat16 [32768, 4096], P('sp', 'tp'), may hold values from -6 to 6
- norm_gain: float32 [4096], replicated, may hold values from 0.1 to 1.9
- pool_in_weight: bfloat16 [4096, 2048], P('sp', 'tp'), may hold values from -0.09375 to 0.09375
- query_weight: bfloat16 [4096, 2048], P('sp', 'tp'), may hold values from -1 to 1, as said below
- key_weight: bfloat16 [4096, 512], P('sp', 'tp'), may hold values from -40 to 40
- value_weight: bfloat16 [4096, 512], P('sp', 'tp'), may hold values from -0.09375 to 0.09375
- pool_weight: bfloat16 [8, 256, 256], P('tp'), may hold values from -0.375 to 0.375
- pool_scale: float32 [2048], P('tp'), may hold values from 0.1 to 1.9
- sink_logit: float32 [32], P('tp'), may hold values from 3 to 7
- out_pool_weight: bfloat16 [2048, 4096], P('tp', 'sp'), may hold values from -0.09375 to 0.09375
- out_attn_weight: bfloat16 [2048, 4096], P('tp', 'sp'), may hold values from -1.5 to 1.5
Outputs:
- mixed: bfloat16 [32768, 4096], P(('sp', 'tp'))
Inputs may be any that keep to these rules, and one draw needn't show every extreme that they name: `query_weight`: entries of order 4096 ** -0.5, drawn independently.
All inputs are finite; a program needn't handle non-finite values.
Results may differ from a plain program's by a relative error of at most 0.014.
The roundings to bfloat16 on the way count: a program that leaves them out, or rounds other values in their place, can miss the bound.
Values may be sent and summed in bfloat16 or wider, within the bound.
No kernel may reach another device: no remote copies, remote signals or barrier semaphores. Data moves between devices by JAX's collectives and lax.ppermute only.
A program may use at most 128 MiB of HBM per device.

v0:
```python
import jax
import jax.numpy as jnp
from jax import lax
from jax.sharding import Mesh
from jax.sharding import PartitionSpec as P

HEAD_DIM = 64
Q_HEADS = 32
KV_HEADS = 8
GROUP_DIM = 256
WINDOW = 128
GRID_W = 64
SP = ("sp_0", "sp_1")
SP_TP = ("sp_0", "sp_1", "tp")
epsilon = 1e-06
rotary_base = 10000.0
masked_score = -1e30


def sent_together(arrays, axis, dim, along):
    widths = [a.shape[along] for a in arrays]
    both = jnp.concatenate(arrays, axis=along)
    result = lax.all_gather(both, axis, axis=dim, tiled=True)
    return tuple(jnp.split(result, [sum(widths[:k]) for k in range(1, len(widths))], axis=along))


def padded_2(block, sides, width):
    for axis, dim in sides:
        count = lax.axis_size(axis)
        forward = [(i, i + 1) for i in range(count - 1)]
        backward = [(target, source) for source, target in forward]
        low = lax.ppermute(
            lax.slice_in_dim(block, block.shape[dim] - width, None, axis=dim), axis, forward
        )
        high = lax.ppermute(lax.slice_in_dim(block, 0, width, axis=dim), axis, backward)
        block = jnp.concatenate([low, block, high], axis=dim)
    return block


def gather_axes(array, axes, dim):
    if not axes:
        return array
    nearer = lax.all_gather(array, axes[-1], axis=dim, tiled=True)
    return gather_axes(nearer, axes[:-1], dim)


def rms_normed(values, gain):
    floats = values.astype(jnp.float32)
    scaled = floats * lax.rsqrt(jnp.mean(floats * floats, axis=-1, keepdims=True) + epsilon)
    return (scaled * gain).astype(jnp.bfloat16)


def rotary_tables(positions, head_dim, grid_width):
    freq_count = head_dim // 4
    inverse = rotary_base ** (-jnp.arange(freq_count, dtype=jnp.float32) / freq_count)
    row_pos = (positions // grid_width).astype(jnp.float32)
    col_pos = (positions % grid_width).astype(jnp.float32)
    angles = jnp.stack([row_pos[:, None] * inverse, col_pos[:, None] * inverse], axis=1)
    return (jnp.cos(angles), jnp.sin(angles))


def rotate(values, cosine, sine):
    length, heads, head_dim = values.shape
    split = values.reshape(length, heads, 2, 2, head_dim // 4)
    first = split[:, :, :, 0]
    second = split[:, :, :, 1]
    cos_b = cosine[:, None]
    sin_b = sine[:, None]
    turned = jnp.stack([first * cos_b - second * sin_b, second * cos_b + first * sin_b], axis=3)
    return turned.reshape(length, heads, head_dim)


def shards(
    tokens,
    norm_gain,
    pool_in_weight,
    query_weight,
    key_weight,
    value_weight,
    pool_weight,
    pool_scale,
    sink_logit,
    out_pool_weight,
    out_attn_weight,
):
    whole_rows = lax.all_gather(tokens, "tp", axis=1, tiled=True)
    normed = rms_normed(whole_rows, norm_gain)
    tok_rows = normed.shape[0]

    def project(piece):
        return jnp.dot(normed, piece, preferred_element_type=jnp.float32)

    pieces = sent_together((pool_in_weight, query_weight, key_weight, value_weight), SP, 0, 1)
    pool_raw, query_raw, key_raw, value_raw = tuple((project(piece) for piece in pieces))
    sp_index = lax.axis_index(SP)
    tp_index = lax.axis_index("tp")
    total_rows = tok_rows * lax.axis_size(SP)
    offset = sp_index * tok_rows
    positions = offset + jnp.arange(tok_rows, dtype=jnp.int32)
    cosine, sine = rotary_tables(positions, HEAD_DIM, GRID_W)
    pool_in = pool_raw.astype(jnp.bfloat16)
    queries = rotate(query_raw.reshape(tok_rows, -1, HEAD_DIM), cosine, sine).astype(jnp.bfloat16)
    key_part = rotate(key_raw.reshape(tok_rows, -1, HEAD_DIM), cosine, sine).astype(jnp.bfloat16)
    key_part = key_part.reshape(tok_rows, -1)
    value_part = value_raw.astype(jnp.bfloat16)
    kv_rows = jnp.concatenate([key_part, value_part], axis=1)
    kv_width = key_part.shape[1]
    channels = pool_in.shape[1]
    pool_reach = 8
    rim_depth = max(WINDOW, pool_reach)
    padded = padded_2(jnp.concatenate([pool_in, kv_rows], axis=1), ((SP, 0),), rim_depth)
    pool_pad = padded[rim_depth - pool_reach : rim_depth + tok_rows + pool_reach, :channels]
    kv_pad = padded[rim_depth - WINDOW : rim_depth + tok_rows + WINDOW, channels:]
    running = jnp.concatenate(
        [jnp.zeros((1, channels), jnp.float32), jnp.cumsum(pool_pad.astype(jnp.float32), axis=0)],
        axis=0,
    )
    groups_dev = channels // GROUP_DIM
    selector = (tp_index * groups_dev + jnp.arange(channels, dtype=jnp.int32) // GROUP_DIM) % 4
    window_mean = jnp.zeros((tok_rows, channels), jnp.float32)
    for level, half_width in enumerate((1, 2, 4, 8)):
        window_sum = (
            running[pool_reach + half_width : pool_reach + half_width + tok_rows]
            - running[pool_reach - half_width : pool_reach - half_width + tok_rows]
        )
        counts = jnp.minimum(positions + half_width, total_rows) - jnp.maximum(
            positions - half_width, 0
        )
        level_mean = window_sum / counts.astype(jnp.float32)[:, None]
        window_mean = jnp.where((selector == level)[None, :], level_mean, window_mean)
    pooled = (window_mean - pool_in.astype(jnp.float32)).astype(jnp.bfloat16)
    mixing = jnp.einsum(
        "tgc,gcd->tgd",
        pooled.reshape(tok_rows, groups_dev, GROUP_DIM),
        pool_weight,
        preferred_element_type=jnp.float32,
    )
    pool_out = (mixing.reshape(tok_rows, channels) * pool_scale).astype(jnp.bfloat16)
    group = Q_HEADS // KV_HEADS
    kv_heads_dev = kv_width // HEAD_DIM
    query_groups = queries.reshape(tok_rows, kv_heads_dev, group, HEAD_DIM)
    key_pad = kv_pad[:, :kv_width].reshape(-1, kv_heads_dev, HEAD_DIM)
    value_pad = kv_pad[:, kv_width:].reshape(-1, kv_heads_dev, HEAD_DIM)
    scores = jnp.einsum(
        "qkgd,skd->kgqs", query_groups, key_pad, preferred_element_type=jnp.float32
    ) * HEAD_DIM ** (-0.5)
    key_pos = offset - WINDOW + jnp.arange(tok_rows + 2 * WINDOW, dtype=jnp.int32)
    allowed = (
        (jnp.abs(key_pos[None, :] - positions[:, None]) <= WINDOW)
        & (key_pos >= 0)[None, :]
        & (key_pos < total_rows)[None, :]
    )
    scores = jnp.where(allowed, scores, masked_score)
    sink = sink_logit.reshape(kv_heads_dev, group, 1, 1)
    highest = jnp.maximum(jnp.max(scores, axis=-1, keepdims=True), sink)
    expo = jnp.exp(scores - highest)
    denominator = jnp.sum(expo, axis=-1, keepdims=True) + jnp.exp(sink - highest)
    weights = (expo / denominator).astype(jnp.bfloat16)
    attended = jnp.einsum("kgqs,skd->qkgd", weights, value_pad, preferred_element_type=jnp.float32)
    attn_out = attended.reshape(tok_rows, -1).astype(jnp.bfloat16)
    out_pool_full, out_attn_full = (
        gather_axes(out_pool_weight, SP, 1),
        gather_axes(out_attn_weight, SP, 1),
    )
    return lax.psum_scatter(
        (
            jnp.dot(pool_out, out_pool_full, preferred_element_type=jnp.float32)
            + jnp.dot(attn_out, out_attn_full, preferred_element_type=jnp.float32)
        ).astype(jnp.bfloat16),
        "tp",
        scatter_dimension=0,
        tiled=True,
    )


def solution(mesh):
    finer = Mesh(mesh.devices.reshape(8, 4, mesh.shape["tp"]), ("sp_0", "sp_1", "tp"))
    return jax.shard_map(
        shards,
        mesh=finer,
        in_specs=(
            P(SP, "tp"),
            P(),
            P(SP, "tp"),
            P(SP, "tp"),
            P(SP, "tp"),
            P(SP, "tp"),
            P("tp", None, None),
            P("tp"),
            P("tp"),
            P("tp", SP),
            P("tp", SP),
        ),
        out_specs=P(SP_TP, None),
        check_vma=False,
    )
```

profile of v0, /device:TPU:1, one launch (start us, length us, event | category | flops | bytes accessed | tf_op | source)
XLA Modules:
  0.0 306.1 jit_solution(10103627928105953874)
XLA Ops:
  9.0 1.6 pad_maximum_fusion.2
  10.7 12.0 %all_gather.20 = bf16[256,512]{1,0:T(8,128)(2,1)} all-gather(bf16[256,128]{1,0:T(8,128)(2,1)} %param.20), channel_id=1, replica_groups=mesh['sp_0'=8,'sp_1'=4,'tp'=8] {'sp_1'}, dimensions={1}, use_global_device_ids=true | all-gather | bytes 327680 | tf_op jit(solution)/shard_map/all_gather | solution.py:43
  22.7 11.1 %all_gather.22 = bf16[256,512]{1,0:T(8,128)(2,1)} all-gather(bf16[256,128]{1,0:T(8,128)(2,1)} %param.21), channel_id=1, replica_groups=mesh['sp_0'=8,'sp_1'=4,'tp'=8] {'sp_1'}, dimensions={1}, use_global_device_ids=true | all-gather | bytes 327680 | tf_op jit(solution)/shard_map/all_gather | solution.py:43
  35.7 3.1 fusion.7
  38.8 26.8 %all-gather.5.cloned.1.call-done = bf16[1024,4096]{1,0:T(8,128)(2,1)} async-done(((bf16[1024,512]{1,0:T(8,128)(2,1)}), bf16[1024,4096]{1,0:T(8,128)(2,1)}) %all-gather.5.cloned.1.call-update) | async-done | bytes 8388624 | tf_op jit(solution)/shard_map/all_gather | solution.py:86
  65.6 5.1 %fusion.1 = f32[1024]{0:T(1024)S(1)} fusion(bf16[1024,4096]{1,0:T(8,128)(2,1)} %all-gather.5.cloned.1.call-done), kind=kLoop, calls=%fused_computation.6 | loop fusion | flops 12581888 | bytes 8392704 | tf_op jit(solution)/shard_map/reduce_sum | solution.py:49
  70.7 10.3 %fusion.3 = bf16[1024,4096]{1,0:T(8,128)(2,1)} fusion(bf16[1024,4096]{1,0:T(8,128)(2,1)} %all-gather.5.cloned.1.call-done, f32[4096]{0:T(1024)S(1)} %copy-done.13, f32[1024]{0:T(1024)S(1)} %add_rsqrt_fusion), kind=kLoop, calls=%fused_computation.8 | loop fusion | flops 16777216 | bytes 16797696 | tf_op jit(solution)/shard_map/convert_element_type | solution.py:50
  81.0 68.8 %all-gather.7.cloned.1.call-done = bf16[4096,640]{1,0:T(8,128)(2,1)} async-done(((bf16[128,640]{1,0:T(8,128)(2,1)}), bf16[4096,640]{1,0:T(8,128)(2,1)}) %all-gather.7.cloned.1.call-update) | async-done | bytes 5242896 | tf_op jit(solution)/shard_map/all_gather | solution.py:23
  149.9 6.4 %fusion.33 = f32[1024,64]{0,1:T(8,128)S(1)} fusion(bf16[1024,4096]{1,0:T(8,128)(2,1)} %fusion.3, bf16[4096,640]{1,0:T(8,128)(2,1)} %all-gather.7.cloned.1.call-done), kind=kOutput, calls=%fused_computation.42 | convolution fusion | flops 536870912 | bytes 9699328 | tf_op jit(solution)/shard_map/dot_general | solution.py:91
  157.4 2.4 fusion.14
  159.8 2.7 convolution_convert_fusion
  162.6 1.9 collective-permute-start
  164.5 1.5 collective-permute-start.1
  166.0 2.4 fusion.8
  171.6 1.3 fusion.12
  173.2 5.2 %fusion.96 = (f32[4,1024]{1,0:T(4,128)S(1)}, f32[1,4,1024,1280]{2,3,1,0:T(8,128)S(1)}) fusion(bf16[1024,4,64]{0,2,1:T(8,128)(2,1)} %bitcast.62, bf16[128,384]{0,1:T(8,128)(2,1)} %copy-done.11, bf16[128,384]{0,1:T(8,128)(2,1)} %copy-done.9, bf16[1024,64]{0,1:T(8,128)(2,1)S(1)} %convolution_convert_fusion, bf16[1024,64]{0,1:T(8,128)(2,1)} %bitcast.59, ...), kind=kOutput, calls=%fused_computation.140 | convolution fusion | flops 687632384 | bytes 23805952 | tf_op jit(solution)/shard_map/qkgd,skd->kgqs/dot_general | solution.py:144
  178.5 3.0 fusion
  181.5 4.0 %copy-done.3 = f32[1,4,1024,1280]{2,3,1,0:T(8,128)} copy-done((f32[1,4,1024,1280]{2,3,1,0:T(8,128)}, f32[1,4,1024,1280]{2,3,1,0:T(8,128)S(1)}, u32[]{:S(2)}) %copy-start.3) | copy-done | bytes 20971544
  186.7 3.0 all-gather.9.cloned.1.call-done
  189.8 10.7 %fusion.21 = f32[1024,4096]{1,0:T(8,128)} fusion(bf16[256,4096]{1,0:T(8,128)(2,1)} %all-gather.9.cloned.1.call-done, bf16[1024,256]{0,1:T(8,128)(2,1)S(1)} %copy-done.5, f32[1152,256]{0,1:T(8,128)S(1)} %bitcast.55, f32[1040,256]{0,1:T(8,128)S(1)} %bitcast.56, f32[256]{0:T(256)S(1)} %copy-done.15, f32[1024]{0:T(1024)S(1)} %get-tuple-element.23, ...), kind=kOutput, calls=%fused_computation.25 | convolution fusion | flops 2286157824 | bytes 28068864 | tf_op jit(solution)/shard_map/dot_general | solution.py:167
  200.5 9.3 %fusion.18 = bf16[64,4,1024]{2,0,1:T(8,128)(2,1)S(1)} fusion(f32[4,1024]{1,0:T(4,128)S(1)} %exponential_add_fusion, f32[1,4,1024,1280]{2,3,1,0:T(8,128)} %copy-done.3, f32[4,1024]{1,0:T(4,128)S(1)} %broadcast_maximum_fusion, bf16[128,384]{0,1:T(8,128)(2,1)S(1)} %copy-done.12, bf16[128,384]{0,1:T(8,128)(2,1)S(1)} %copy-done.10, ...), kind=kOutput, calls=%fused_computation.24 | convolution fusion | flops 687898624 | bytes 22511616 | tf_op jit(solution)/shard_map/kgqs,skd->qkgd/dot_general | solution.py:159
  209.8 20.3 %all-gather.11.cloned.1.call-done = bf16[256,4096]{1,0:T(8,128)(2,1)} async-done(((bf16[256,512]{1,0:T(8,128)(2,1)}), bf16[256,4096]{1,0:T(8,128)(2,1)}) %all-gather.11.cloned.1.call-update) | async-done | bytes 2097168 | tf_op jit(solution)/shard_map/all_gather | solution.py:43
  230.1 12.1 %add_convert_fusion = bf16[1024,4096]{1,0:T(8,128)(2,1)} fusion(f32[1024,4096]{1,0:T(8,128)} %fusion.21, bf16[1024,256]{0,1:T(8,128)(2,1)S(1)} %bitcast.54, bf16[256,4096]{1,0:T(8,128)(2,1)} %all-gather.11.cloned.1.call-done), kind=kOutput, calls=%fused_computation.9 | convolution fusion | flops 2155872256 | bytes 27787264 | tf_op jit(solution)/shard_map/dot_general | solution.py:168
  242.2 57.4 %reduce-scatter.2.cloned.1.call-done = bf16[128,4096]{1,0:T(8,128)(2,1)} async-done(((bf16[1024,4096]{1,0:T(8,128)(2,1)}), bf16[128,4096]{1,0:T(8,128)(2,1)}) %reduce-scatter.2.cloned.1.call-update) | async-done | bytes 1048592 | tf_op jit(solution)/shard_map/reduce_scatter | solution.py:165
  (81 shorter events, 10.3 us)
Async XLA Ops:
  6.5 183.2 %copy-start = (bf16[1,256,256]{2,1,0:T(8,128)(2,1)S(1)}, bf16[1,256,256]{2,1,0:T(8,128)(2,1)}, u32[]{:S(2)}) copy-start(bf16[1,256,256]{2,1,0:T(8,128)(2,1)} %param.17) | copy-start | bytes 393220
  6.5 59.1 %all-gather.5.cloned.1.call-start = ((), (), s32[]{:S(2)}) async-start(), calls=%async_computation.1 | async-start | bytes 9437184 | tf_op jit(solution)/shard_map/all_gather | solution.py:86
  7.3 142.6 %all-gather.7.cloned.1.call-start = ((), (), s32[]{:S(2)}) async-start(), calls=%async_computation.2 | async-start | bytes 5406720 | tf_op jit(solution)/shard_map/all_gather | solution.py:23
  10.6 179.1 %all-gather.9.cloned.1.call-start = ((), (), s32[]{:S(2)}) async-start(), calls=%async_computation.3 | async-start | bytes 2359296 | tf_op jit(solution)/shard_map/all_gather | solution.py:43
  22.7 207.4 %all-gather.11.cloned.1.call-start = ((), (), s32[]{:S(2)}) async-start(), calls=%async_computation.4 | async-start | bytes 2359296 | tf_op jit(solution)/shard_map/all_gather | solution.py:43
  33.8 36.9 %copy-start.13 = (f32[4096]{0:T(1024)S(1)}, f32[4096]{0:T(1024)}, u32[]{:S(2)}) copy-start(f32[4096]{0:T(1024)} %param.12) | copy-start | bytes 49156
  33.8 265.8 %reduce-scatter.2.cloned.1.call-start = ((), (), s32[]{:S(2)}) async-start(), calls=%async_computation.5 | async-start | bytes 9437184 | tf_op jit(solution)/shard_map/reduce_scatter | solution.py:165
  149.8 6.9 %copy-start.2 = (bf16[1024,4096]{1,0:T(8,128)(2,1)S(1)}, bf16[1024,4096]{1,0:T(8,128)(2,1)}, u32[]{:S(2)}) copy-start(bf16[1024,4096]{1,0:T(8,128)(2,1)} %fusion.3) | copy-start | bytes 25165828
  149.9 7.6 %copy-start.8 = (bf16[4096,640]{1,0:T(8,128)(2,1)S(1)}, bf16[4096,640]{1,0:T(8,128)(2,1)}, u32[]{:S(2)}) copy-start(bf16[4096,640]{1,0:T(8,128)(2,1)} %all-gather.7.cloned.1.call-done) | copy-start | bytes 15728644
  157.4 12.8 %copy-start.6 = (bf16[1024,1,2,2,16]{0,4,3,2,1:T(8,128)(2,1)}, bf16[1024,1,2,2,16]{0,4,3,2,1:T(8,128)(2,1)S(1)}, u32[]{:S(2)}) copy-start(bf16[1024,1,2,2,16]{0,4,3,2,1:T(8,128)(2,1)S(1)} %pad_maximum_fusion.4) | copy-start | bytes 393220
  159.8 10.4 %copy-start.4 = (bf16[1024,256]{0,1:T(8,128)(2,1)}, bf16[1024,256]{0,1:T(8,128)(2,1)S(1)}, u32[]{:S(2)}) copy-start(bf16[1024,256]{0,1:T(8,128)(2,1)S(1)} %fusion.14) | copy-start | bytes 1572868
  162.6 6.8 %collective-permute-start = (bf16[128,384]{0,1:T(8,128)(2,1)S(1)}, bf16[128,384]{0,1:T(8,128)(2,1)S(1)}, u32[]{:S(2)}, u32[]{:S(2)}) collective-permute-start(bf16[128,384]{0,1:T(8,128)(2,1)S(1)} %get-tuple-element.7), channel_id=1, source_target_pairs={{0,8},{8,16},{16,24},{24,32},{32,40},{40,48},{48,56},{56,64},{64,7... | collective-permute-start | bytes 294920 | tf_op jit(solution)/shard_map/ppermute | solution.py:32
  164.5 5.8 %collective-permute-start.1 = (bf16[128,384]{0,1:T(8,128)(2,1)S(1)}, bf16[128,384]{0,1:T(8,128)(2,1)S(1)}, u32[]{:S(2)}, u32[]{:S(2)}) collective-permute-start(bf16[128,384]{0,1:T(8,128)(2,1)S(1)} %get-tuple-element.8), channel_id=1, source_target_pairs={{8,0},{16,8},{24,16},{32,24},{40,32},{48,40},{56,48},{64,56},{72,6... | collective-permute-start | bytes 294920 | tf_op jit(solution)/shard_map/ppermute | solution.py:35
  173.2 5.2 %copy-start.14 = (f32[4]{0:T(128)S(1)}, f32[4]{0:T(128)}, u32[]{:S(2)}) copy-start(f32[4]{0:T(128)} %param.19) | copy-start | bytes 52
  178.4 7.1 %copy-start.3 = (f32[1,4,1024,1280]{2,3,1,0:T(8,128)}, f32[1,4,1024,1280]{2,3,1,0:T(8,128)S(1)}, u32[]{:S(2)}) copy-start(f32[1,4,1024,1280]{2,3,1,0:T(8,128)S(1)} %get-tuple-element.20) | copy-start | bytes 62914564
  185.5 4.2 %copy-start.5 = (bf16[1024,256]{0,1:T(8,128)(2,1)S(1)}, bf16[1024,256]{0,1:T(8,128)(2,1)}, u32[]{:S(2)}) copy-start(bf16[1024,256]{0,1:T(8,128)(2,1)} %copy-done.4) | copy-start | bytes 1572868
  185.5 4.2 %copy-start.15 = (f32[256]{0:T(256)S(1)}, f32[256]{0:T(256)}, u32[]{:S(2)}) copy-start(f32[256]{0:T(256)} %param.18) | copy-start | bytes 3076
  185.5 4.2 %copy-start.16 = (pred[256]{0:T(512)(128)(4,1)S(1)}, pred[256]{0:T(512)(128)(4,1)}, u32[]{:S(2)}) copy-start(pred[256]{0:T(512)(128)(4,1)} %get-tuple-element.27) | copy-start | bytes 772
  185.5 4.2 %copy-start.17 = (pred[256]{0:T(512)(128)(4,1)S(1)}, pred[256]{0:T(512)(128)(4,1)}, u32[]{:S(2)}) copy-start(pred[256]{0:T(512)(128)(4,1)} %get-tuple-element.28) | copy-start | bytes 772
  185.6 4.2 %copy-start.18 = (pred[256]{0:T(512)(128)(4,1)S(1)}, pred[256]{0:T(512)(128)(4,1)}, u32[]{:S(2)}) copy-start(pred[256]{0:T(512)(128)(4,1)} %get-tuple-element.29) | copy-start | bytes 772
  189.8 10.7 %copy-start.7 = (bf16[1024,1,2,2,16]{0,4,3,2,1:T(8,128)(2,1)S(1)}, bf16[1024,1,2,2,16]{0,4,3,2,1:T(8,128)(2,1)}, u32[]{:S(2)}) copy-start(bf16[1024,1,2,2,16]{0,4,3,2,1:T(8,128)(2,1)} %copy-done.6) | copy-start | bytes 393220
  189.8 10.7 %copy-start.10 = (bf16[128,384]{0,1:T(8,128)(2,1)S(1)}, bf16[128,384]{0,1:T(8,128)(2,1)}, u32[]{:S(2)}) copy-start(bf16[128,384]{0,1:T(8,128)(2,1)} %copy-done.9) | copy-start | bytes 294916
  189.8 10.7 %copy-start.12 = (bf16[128,384]{0,1:T(8,128)(2,1)S(1)}, bf16[128,384]{0,1:T(8,128)(2,1)}, u32[]{:S(2)}) copy-start(bf16[128,384]{0,1:T(8,128)(2,1)} %copy-done.11) | copy-start | bytes 294916
  230.1 69.5 %copy-start.1 = (bf16[1,256,256]{2,1,0:T(8,128)(2,1)S(1)}, bf16[1,256,256]{2,1,0:T(8,128)(2,1)}, u32[]{:S(2)}) copy-start(bf16[1,256,256]{2,1,0:T(8,128)(2,1)} %param.17) | copy-start | bytes 393220
  (3 other events, 5.8 us)
Sparse Core Ops, SparseCore 0:
  9.2 56.4 all-gather.4
  68.2 81.6 all-gather.6
  151.6 38.0 all-gather.8
  191.4 38.6 all-gather.10
  242.3 57.2 reduce-scatter.1
where the time goes:
time: 307 us; the launch traced here: 306 us
  waiting for transfers between devices  178 us (58%)
  matrix products  51.3 us (17%)
  other arithmetic  28.3 us (9%)
  blocking collectives  23 us (7%)
  between operations  13.5 us (4%)
  local copies, waits for them, and re-layouts  8.52 us (3%)
  starting transfers between devices  3.52 us (1%)
    all_gather x1, waiting for transfers between devices, sent_together(): result = lax.all_gather(both, axis, axis=dim, tiled=True)  68.8 us
    reduce_scatter x1, waiting for transfers between devices, shards(): lax.psum_scatter((jnp.dot(pool_out, out_pool_full, preferred_element_type...  57.4 us
    all_gather x1, waiting for transfers between devices, shards(): whole_rows = lax.all_gather(tokens, 'tp', axis=1, tiled=True)  26.8 us
    all_gather x2, waiting for transfers between devices, gather_axes(): nearer = lax.all_gather(array, axes[-1], axis=dim, tiled=True)  23.3 us
    all_gather x2, blocking collectives, gather_axes(): nearer = lax.all_gather(array, axes[-1], axis=dim, tiled=True)  23 us
    dot_general x4, matrix products, project(): return jnp.dot(normed, piece, preferred_element_type=jnp.float32)  13.9 us
    dot_general x1, matrix products, shards(): jnp.dot(attn_out, out_attn_full, preferred_element_type=jnp.float32)  12.1 us
    dot_general x1, matrix products, shards(): jnp.dot(pool_out, out_pool_full, preferred_element_type=jnp.float32)  10.7 us
  transfers between devices with their start and end apart: 7, of which 6 were waited for; matrix products, arithmetic and copies ran while one was open for 23% of the time, Pallas kernels for 0%

commit v1 on v0

--- a/solution.py
+++ b/solution.py
@@ -83,7 +83,14 @@
     out_pool_weight,
     out_attn_weight,
 ):
-    whole_rows = lax.all_gather(tokens, "tp", axis=1, tiled=True)
+
+    def spread_thing_by_axis(axis_key, work_x):
+        nodes = jax.lax.axis_size(axis_key)
+        block_list = tuple((nodes if p == 1 else 1 for p in range(work_x.ndim)))
+        met_up = jnp.tile(work_x, block_list)
+        return jax.lax.all_to_all(met_up, axis_key, split_axis=1, concat_axis=1, tiled=True)
+
+    whole_rows = spread_thing_by_axis("tp", tokens)
     normed = rms_normed(whole_rows, norm_gain)
     tok_rows = normed.shape[0]
 

time: 307 us -> 286 us (0.932)
  waiting for transfers between devices: 178 us -> 128 us
  local copies, waits for them, and re-layouts: 8.52 us -> 31.4 us
  starting transfers between devices: 3.52 us -> 11.3 us
    all_gather x1, waiting for transfers between devices: 68.8 us -> 0.01 us  [sent_together(): result = lax.all_gather(both, axis, axis=dim, tiled=True)]
    all_to_all x0 -> x1, waiting for transfers between devices: none -> 67.3 us  [spread_thing_by_axis(): jax.lax.all_to_all(met_up, axis_key, split_axis=1, concat_axis=1, tiled=T...]
    all_gather x1 -> x0, waiting for transfers between devices: 26.8 us -> none  [shards(): whole_rows = lax.all_gather(tokens, 'tp', axis=1, tiled=True)]
    all_gather x2, waiting for transfers between devices: 23.3 us -> 0.04 us  [gather_axes(): nearer = lax.all_gather(array, axes[-1], axis=dim, tiled=True)]
    all_to_all x0 -> x1, local copies, waits for them, and re-layouts: none -> 11.6 us  [spread_thing_by_axis(): jax.lax.all_to_all(met_up, axis_key, split_axis=1, concat_axis=1, tiled=T...]
    all_to_all x0 -> x1, starting transfers between devices: none -> 8.17 us  [spread_thing_by_axis(): jax.lax.all_to_all(met_up, axis_key, split_axis=1, concat_axis=1, tiled=T...]
    dot_general x0 -> x4, local copies, waits for them, and re-layouts: none -> 6.36 us  [project(): return jnp.dot(normed, piece, preferred_element_type=jnp.float32)]
    another operation x5 -> x6, local copies, waits for them, and re-layouts: 1.67 us -> 6.86 us  [the longest x1 5.19 us: spread_thing_by_axis(): met_up = jnp.tile(work_x, block_list)]
  transfers between devices with their start and end apart: 7 -> 7, of which waited for: 6 -> 3; matrix products, arithmetic and copies ran while one was open for 23% -> 32% of each run, Pallas kernels for 0% -> 0%
where the time goes in v1:
time: 286 us; the launch traced here: 285 us
  waiting for transfers between devices  128 us (45%)
  matrix products  52.6 us (18%)
  local copies, waits for them, and re-layouts  31.4 us (11%)
  other arithmetic  26.9 us (9%)
  blocking collectives  21.2 us (7%)
  between operations  13.7 us (5%)
  starting transfers between devices  11.3 us (4%)
    all_to_all x1, waiting for transfers between devices, spread_thing_by_axis(): jax.lax.all_to_all(met_up, axis_key, split_axis=1, concat_axis=1, tiled=T...  67.3 us
    reduce_scatter x1, waiting for transfers between devices, shards(): lax.psum_scatter((jnp.dot(pool_out, out_pool_full, preferred_element_type...  59.2 us
    all_gather x2, blocking collectives, gather_axes(): nearer = lax.all_gather(array, axes[-1], axis=dim, tiled=True)  21.2 us
    dot_general x4, matrix products, project(): return jnp.dot(normed, piece, preferred_element_type=jnp.float32)  15.5 us
    dot_general x1, matrix products, shards(): jnp.dot(attn_out, out_attn_full, preferred_element_type=jnp.float32)  12.1 us
    all_to_all x1, local copies, waits for them, and re-layouts, spread_thing_by_axis(): jax.lax.all_to_all(met_up, axis_key, split_axis=1, concat_axis=1, tiled=T...  11.6 us
    dot_general x1, matrix products, shards(): jnp.dot(pool_out, out_pool_full, preferred_element_type=jnp.float32)  10.7 us
    dot_general x1, matrix products, shards(): jnp.einsum('kgqs,skd->qkgd', weights, value_pad, preferred_element_type=j...  9.21 us
  transfers between devices with their start and end apart: 7, of which 3 were waited for; matrix products, arithmetic and copies ran while one was open for 32% of the time, Pallas kernels for 0%

profile of v1, /device:TPU:1, one launch (start us, length us, event | category | flops | bytes accessed | tf_op | source)
XLA Modules:
  0.0 284.7 jit_solution(9733461760105701471)
XLA Ops:
  8.2 1.6 pad_maximum_fusion.2
  9.9 5.2 %tile.2 = bf16[1024,8,512]{2,0,1:T(8,128)(2,1)} broadcast(bf16[1024,512]{1,0:T(8,128)(2,1)} %param.11), dimensions={0,2} | broadcast | bytes 9437184 | tf_op jit(solution)/shard_map/tile | solution.py:90
  15.1 8.2 %all-to-all-start = ((bf16[1024,8,512]{2,0,1:T(8,128)(2,1)}), bf16[1024,8,512]{2,0,1:T(8,128)(2,1)}, u32[]{:S(2)}, u32[]{:S(2)}) async-start(bf16[1024,8,512]{2,0,1:T(8,128)(2,1)} %tile.2), calls=%async_computation | async-start | bytes 16777216 | tf_op jit(solution)/shard_map/all_to_all | solution.py:91
  23.3 10.3 %all_gather.16 = bf16[256,512]{1,0:T(8,128)(2,1)} all-gather(bf16[256,128]{1,0:T(8,128)(2,1)S(1)} %copy-done.12), channel_id=1, replica_groups=mesh['sp_0'=8,'sp_1'=4,'tp'=8] {'sp_1'}, dimensions={1}, use_global_device_ids=true | all-gather | bytes 327680 | tf_op jit(solution)/shard_map/all_gather | solution.py:43
  33.7 10.9 %all_gather.18 = bf16[256,512]{1,0:T(8,128)(2,1)} all-gather(bf16[256,128]{1,0:T(8,128)(2,1)S(1)} %copy-done.13), channel_id=1, replica_groups=mesh['sp_0'=8,'sp_1'=4,'tp'=8] {'sp_1'}, dimensions={1}, use_global_device_ids=true | all-gather | bytes 327680 | tf_op jit(solution)/shard_map/all_gather | solution.py:43
  46.5 3.1 %fusion.6 = pred[1024,1280]{0,1:T(8,128)(4,1)} fusion(s32[1024]{0:T(1024)S(1)} %iota_add_fusion.1, s32[1280]{0:T(1024)S(1)} %iota_add_fusion, pred[1280]{0:T(1024)(128)(4,1)S(1)} %get-tuple-element.31, pred[1280]{0:T(1024)(128)(4,1)S(1)} %get-tuple-element.32), kind=kLoop, calls=%fused_computation.14 | loop fusion | flops 6553600 | bytes 1322496 | tf_op jit(solution)/shard_map/and | solution.py:156
  49.7 67.3 %all-to-all-done = bf16[1024,8,512]{2,0,1:T(8,128)(2,1)} async-done(((bf16[1024,8,512]{2,0,1:T(8,128)(2,1)}), bf16[1024,8,512]{2,0,1:T(8,128)(2,1)}, u32[]{:S(2)}, u32[]{:S(2)}) %all-to-all-start) | async-done | bytes 8388640 | tf_op jit(solution)/shard_map/all_to_all | solution.py:91
  117.0 11.6 %copy.37 = bf16[1024,8,512]{0,2,1:T(8,128)(2,1)} copy(bf16[1024,8,512]{2,0,1:T(8,128)(2,1)} %all-to-all-done) | data formatting | bytes 16777216 | tf_op jit(solution)/shard_map/all_to_all | solution.py:91
  128.6 5.3 %multiply_reduce_fusion = f32[1024]{0:T(1024)S(1)} fusion(bf16[1024,8,512]{0,2,1:T(8,128)(2,1)} %copy.37), kind=kLoop, calls=%fused_computation.9 | loop fusion | flops 12581888 | bytes 8392704 | tf_op jit(solution)/shard_map/reduce_sum | solution.py:49
  134.4 4.4 %fusion.2 = bf16[1024,4096]{0,1:T(8,128)(2,1)} fusion(bf16[1024,8,512]{0,2,1:T(8,128)(2,1)S(1)} %copy-done.1, f32[4096]{0:T(1024)S(1)} %copy-done.14, f32[1024]{0:T(1024)S(1)} %add_rsqrt_fusion), kind=kLoop, calls=%fused_computation.6 | loop fusion | flops 16777216 | bytes 16797696 | tf_op jit(solution)/shard_map/convert_element_type | solution.py:50
  138.8 4.3 %multiply_convert_fusion = bf16[1024,8,512]{0,2,1:T(8,128)(2,1)} fusion(bf16[1024,8,512]{0,2,1:T(8,128)(2,1)S(1)} %copy-done.1, f32[8,512]{1,0:T(8,128)S(1)} %mul.187, f32[1024]{0:T(1024)S(1)} %add_rsqrt_fusion), kind=kLoop, calls=%fused_computation.8 | loop fusion | flops 16777216 | bytes 16797696 | tf_op jit(solution)/shard_map/convert_element_type | solution.py:50
  143.1 1.7 slice_bitcast_fusion
  144.8 3.0 %copy.46 = bf16[256,4096]{1,0:T(8,128)(2,1)} copy(bf16[256,4096]{0,1:T(8,128)(2,1)S(1)} %slice_bitcast_fusion) | data formatting | bytes 4194304 | tf_op jit(solution)/shard_map/dot_general | solution.py:98
  149.5 5.2 %convolution_bitcast_fusion = f32[1024,1,2,2,16]{0,4,3,2,1:T(8,128)S(1)} fusion(bf16[1024,4096,1,1]{0,1,3,2:T(8,128)(2,1)} %bitcast.70, bf16[2,2,16,4096]{3,2,1,0:T(8,128)(2,1)S(1)} %bitcast.88), kind=kOutput, calls=%fused_computation.26 | convolution fusion | flops 536870912 | bytes 9175040 | tf_op jit(solution)/shard_map/dot_general | solution.py:98
  155.3 6.1 %fusion.11 = bf16[1024,256]{0,1:T(8,128)(2,1)S(1)} fusion(bf16[1024,4096]{0,1:T(8,128)(2,1)} %fusion.2, bf16[4096,640]{1,0:T(8,128)(2,1)S(1)} %bitcast.80), kind=kOutput, calls=%fused_computation.21 | convolution fusion | flops 2147745792 | bytes 11010048 | tf_op jit(solution)/shard_map/dot_general | solution.py:98
  161.4 2.0 convolution_convert_fusion
  166.5 2.3 fusion.92
  173.4 5.1 %fusion.91 = (f32[4,1024]{1,0:T(4,128)S(1)}, f32[1,4,1024,1280]{2,3,1,0:T(8,128)S(1)}) fusion(bf16[1024,4,64]{0,2,1:T(8,128)(2,1)} %bitcast.89, bf16[128,384]{0,1:T(8,128)(2,1)} %copy-done.10, bf16[128,384]{0,1:T(8,128)(2,1)} %copy-done.8, bf16[1024,64]{0,1:T(8,128)(2,1)} %copy-done.6, bf16[1024,64]{0,1:T(8,128)(2,1)S(1)} %bitcast.86, ...), kind=kOutput, calls=%fused_computation.139 | convolution fusion | flops 687632384 | bytes 23805952 | tf_op jit(solution)/shard_map/qkgd,skd->kgqs/dot_general | solution.py:151
  178.7 3.0 %fusion = f32[4,1024]{1,0:T(4,128)S(1)} fusion(f32[1,4,1024,1280]{2,3,1,0:T(8,128)S(1)} %get-tuple-element.20, f32[4,1024]{1,0:T(4,128)S(1)} %broadcast_maximum_fusion), kind=kLoop, calls=%fused_computation.3 | loop fusion | flops 10481664 | bytes 21004288 | tf_op jit(solution)/shard_map/reduce_sum | solution.py:164
  181.7 3.9 %copy-done.2 = f32[1,4,1024,1280]{2,3,1,0:T(8,128)} copy-done((f32[1,4,1024,1280]{2,3,1,0:T(8,128)}, f32[1,4,1024,1280]{2,3,1,0:T(8,128)S(1)}, u32[]{:S(2)}) %copy-start.2) | copy-done | bytes 20971544
  186.9 10.7 %fusion.18 = f32[1024,4096]{1,0:T(8,128)} fusion(bf16[256,4096]{1,0:T(8,128)(2,1)} %all-gather.6.cloned.1.call-done, bf16[1024,256]{0,1:T(8,128)(2,1)S(1)} %copy-done.5, f32[1152,256]{0,1:T(8,128)S(1)} %bitcast.82, f32[1040,256]{0,1:T(8,128)S(1)} %bitcast.83, f32[256]{0:T(256)S(1)} %copy-done.16, f32[1024]{0:T(1024)S(1)} %get-tuple-element.23, ...), kind=kOutput, calls=%fused_computation.24 | convolution fusion | flops 2286157824 | bytes 28068864 | tf_op jit(solution)/shard_map/dot_general | solution.py:174
  197.6 9.2 %fusion.15 = bf16[64,4,1024]{2,0,1:T(8,128)(2,1)S(1)} fusion(f32[4,1024]{1,0:T(4,128)S(1)} %exponential_add_fusion, f32[1,4,1024,1280]{2,3,1,0:T(8,128)} %copy-done.2, f32[4,1024]{1,0:T(4,128)S(1)} %broadcast_maximum_fusion, bf16[128,384]{0,1:T(8,128)(2,1)S(1)} %copy-done.11, bf16[128,384]{0,1:T(8,128)(2,1)S(1)} %copy-done.9, ...), kind=kOutput, calls=%fused_computation.23 | convolution fusion | flops 687898624 | bytes 22511616 | tf_op jit(solution)/shard_map/kgqs,skd->qkgd/dot_general | solution.py:166
  206.9 12.1 %add_convert_fusion = bf16[1024,4096]{1,0:T(8,128)(2,1)} fusion(f32[1024,4096]{1,0:T(8,128)} %fusion.18, bf16[1024,256]{0,1:T(8,128)(2,1)S(1)} %bitcast.81, bf16[256,4096]{1,0:T(8,128)(2,1)} %all-gather.8.cloned.1.call-done), kind=kOutput, calls=%fused_computation.7 | convolution fusion | flops 2155872256 | bytes 27787264 | tf_op jit(solution)/shard_map/dot_general | solution.py:175
  219.0 59.2 %reduce-scatter.2.cloned.1.call-done = bf16[128,4096]{1,0:T(8,128)(2,1)} async-done(((bf16[1024,4096]{1,0:T(8,128)(2,1)}), bf16[128,4096]{1,0:T(8,128)(2,1)}) %reduce-scatter.2.cloned.1.call-update) | async-done | bytes 1048592 | tf_op jit(solution)/shard_map/reduce_scatter | solution.py:172
  (105 shorter events, 15.3 us)
Async XLA Ops:
  6.5 180.3 %copy-start = (bf16[1,256,256]{2,1,0:T(8,128)(2,1)S(1)}, bf16[1,256,256]{2,1,0:T(8,128)(2,1)}, u32[]{:S(2)}) copy-start(bf16[1,256,256]{2,1,0:T(8,128)(2,1)} %param.17) | copy-start | bytes 393220
  6.5 136.6 %all-gather.4.cloned.1.call-start = ((), (), s32[]{:S(2)}) async-start(), calls=%async_computation.2 | async-start | bytes 5406720 | tf_op jit(solution)/shard_map/all_gather | solution.py:23
  15.1 8.2 %copy-start.12 = (bf16[256,128]{1,0:T(8,128)(2,1)S(1)}, bf16[256,128]{1,0:T(8,128)(2,1)}, u32[]{:S(2)}) copy-start(bf16[256,128]{1,0:T(8,128)(2,1)} %param.20) | copy-start | bytes 196612
  15.1 18.6 %copy-start.13 = (bf16[256,128]{1,0:T(8,128)(2,1)S(1)}, bf16[256,128]{1,0:T(8,128)(2,1)}, u32[]{:S(2)}) copy-start(bf16[256,128]{1,0:T(8,128)(2,1)} %param.21) | copy-start | bytes 196612
  15.1 29.6 %copy-start.14 = (f32[4096]{0:T(1024)S(1)}, f32[4096]{0:T(1024)}, u32[]{:S(2)}) copy-start(f32[4096]{0:T(1024)} %param.12) | copy-start | bytes 49156
  15.1 101.9 %all-to-all-start = ((bf16[1024,8,512]{2,0,1:T(8,128)(2,1)}), bf16[1024,8,512]{2,0,1:T(8,128)(2,1)}, u32[]{:S(2)}, u32[]{:S(2)}) async-start(bf16[1024,8,512]{2,0,1:T(8,128)(2,1)} %tile.2), calls=%async_computation | async-start | bytes 16777216 | tf_op jit(solution)/shard_map/all_to_all | solution.py:91
  23.3 163.5 %all-gather.6.cloned.1.call-start = ((), (), s32[]{:S(2)}) async-start(), calls=%async_computation.3 | async-start | bytes 2359296 | tf_op jit(solution)/shard_map/all_gather | solution.py:43
  33.6 173.2 %all-gather.8.cloned.1.call-start = ((), (), s32[]{:S(2)}) async-start(), calls=%async_computation.4 | async-start | bytes 2359296 | tf_op jit(solution)/shard_map/all_gather | solution.py:43
  44.6 233.6 %reduce-scatter.2.cloned.1.call-start = ((), (), s32[]{:S(2)}) async-start(), calls=%async_computation.5 | async-start | bytes 9437184 | tf_op jit(solution)/shard_map/reduce_scatter | solution.py:172
  128.6 5.9 %copy-start.1 = (bf16[1024,8,512]{0,2,1:T(8,128)(2,1)S(1)}, bf16[1024,8,512]{0,2,1:T(8,128)(2,1)}, u32[]{:S(2)}) copy-start(bf16[1024,8,512]{0,2,1:T(8,128)(2,1)} %copy.37) | copy-start | bytes 25165828
  149.2 6.1 %slice-start.4 = ((s8[5242880]{0:T(1024)(128)(4,1)}), s8[1048576]{0:T(1024)(128)(4,1)S(1)}, s32[]{:S(2)}) async-start(s8[5242880]{0:T(1024)(128)(4,1)} %bitcast.79), calls=%async_computation.10 | async-start | bytes 2097152
  149.5 5.7 %slice-start.5 = ((s8[5242880]{0:T(1024)(128)(4,1)}), s8[4194304]{0:T(1024)(128)(4,1)S(1)}, s32[]{:S(2)}) async-start(s8[5242880]{0:T(1024)(128)(4,1)} %bitcast.79), calls=%async_computation.11 | async-start | bytes 8388608
  149.5 11.8 %slice-start.2 = ((s8[8388608]{0:T(1024)(128)(4,1)}), s8[4194304]{0:T(1024)(128)(4,1)S(1)}, s32[]{:S(2)}) async-start(s8[8388608]{0:T(1024)(128)(4,1)} %bitcast.74), calls=%async_computation.8 | async-start | bytes 8388608
  154.7 11.8 %slice-start = ((s8[8388608]{0:T(1024)(128)(4,1)}), s8[4194304]{0:T(1024)(128)(4,1)S(1)}, s32[]{:S(2)}) async-start(s8[8388608]{0:T(1024)(128)(4,1)} %bitcast.71), calls=%async_computation.6 | async-start | bytes 8388608
  155.2 6.1 %slice-start.3 = ((s8[8388608]{0:T(1024)(128)(4,1)}), s8[4194304]{0:T(1024)(128)(4,1)S(1)}, s32[]{:S(2)}) async-start(s8[8388608]{0:T(1024)(128)(4,1)} %bitcast.74), calls=%async_computation.9 | async-start | bytes 8388608
  155.2 11.2 %slice-start.1 = ((s8[8388608]{0:T(1024)(128)(4,1)}), s8[4194304]{0:T(1024)(128)(4,1)S(1)}, s32[]{:S(2)}) async-start(s8[8388608]{0:T(1024)(128)(4,1)} %bitcast.71), calls=%async_computation.7 | async-start | bytes 8388608
  161.4 9.4 %copy-start.4 = (bf16[1024,256]{0,1:T(8,128)(2,1)}, bf16[1024,256]{0,1:T(8,128)(2,1)S(1)}, u32[]{:S(2)}) copy-start(bf16[1024,256]{0,1:T(8,128)(2,1)S(1)} %fusion.11) | copy-start | bytes 1572868
  163.4 7.4 %copy-start.6 = (bf16[1024,64]{0,1:T(8,128)(2,1)}, bf16[1024,64]{0,1:T(8,128)(2,1)S(1)}, u32[]{:S(2)}) copy-start(bf16[1024,64]{0,1:T(8,128)(2,1)S(1)} %convolution_convert_fusion) | copy-start | bytes 393220
  163.4 6.4 %collective-permute-start = (bf16[128,384]{0,1:T(8,128)(2,1)S(1)}, bf16[128,384]{0,1:T(8,128)(2,1)S(1)}, u32[]{:S(2)}, u32[]{:S(2)}) collective-permute-start(bf16[128,384]{0,1:T(8,128)(2,1)S(1)} %get-tuple-element.7), channel_id=1, source_target_pairs={{0,8},{8,16},{16,24},{24,32},{32,40},{40,48},{48,56},{56,64},{64,7... | collective-permute-start | bytes 294920 | tf_op jit(solution)/shard_map/ppermute | solution.py:32
  165.0 5.8 %collective-permute-start.1 = (bf16[128,384]{0,1:T(8,128)(2,1)S(1)}, bf16[128,384]{0,1:T(8,128)(2,1)S(1)}, u32[]{:S(2)}, u32[]{:S(2)}) collective-permute-start(bf16[128,384]{0,1:T(8,128)(2,1)S(1)} %get-tuple-element.8), channel_id=1, source_target_pairs={{8,0},{16,8},{24,16},{32,24},{40,32},{48,40},{56,48},{64,56},{72,6... | collective-permute-start | bytes 294920 | tf_op jit(solution)/shard_map/ppermute | solution.py:35
  178.6 7.0 %copy-start.2 = (f32[1,4,1024,1280]{2,3,1,0:T(8,128)}, f32[1,4,1024,1280]{2,3,1,0:T(8,128)S(1)}, u32[]{:S(2)}) copy-start(f32[1,4,1024,1280]{2,3,1,0:T(8,128)S(1)} %get-tuple-element.20) | copy-start | bytes 62914564
  186.9 10.7 %copy-start.7 = (bf16[1024,64]{0,1:T(8,128)(2,1)S(1)}, bf16[1024,64]{0,1:T(8,128)(2,1)}, u32[]{:S(2)}) copy-start(bf16[1024,64]{0,1:T(8,128)(2,1)} %copy-done.6) | copy-start | bytes 393220
  186.9 10.7 %copy-start.9 = (bf16[128,384]{0,1:T(8,128)(2,1)S(1)}, bf16[128,384]{0,1:T(8,128)(2,1)}, u32[]{:S(2)}) copy-start(bf16[128,384]{0,1:T(8,128)(2,1)} %copy-done.8) | copy-start | bytes 294916
  186.9 10.7 %copy-start.11 = (bf16[128,384]{0,1:T(8,128)(2,1)S(1)}, bf16[128,384]{0,1:T(8,128)(2,1)}, u32[]{:S(2)}) copy-start(bf16[128,384]{0,1:T(8,128)(2,1)} %copy-done.10) | copy-start | bytes 294916
  (10 other events, 19.5 us)
Sparse Core Ops, SparseCore 0:
  10.0 85.5 all-gather.3
  97.4 36.9 all-gather.5
  136.2 40.9 all-gather.7
  219.1 59.0 reduce-scatter.1
